TPU v7x, 32 devices: a whole 2x2x4 slice. The times are simulated.
32 devices in a mesh: sp: 16 (over z, y, core), tp: 2 (over x).
Axes of the slice: x: 2, y: 2, z: 4, core: 2. Of those that a mesh axis runs over, the one named last changes fastest.
Arguments:
- tokens: bfloat16 [12288, 2048], P(('sp', 'tp')), may hold values from -6 to 6
- input_norm_gain: bfloat16 [2048], replicated, may hold values from 0.099609375 to 1.8984375
- convolution_outer_weight: bfloat16 [2048, 1024], P(None, 'tp'), may hold values from -0.125 to 0.125
- convolution_inner_weight: bfloat16 [2048, 1024], P(None, 'tp'), may hold values from -0.125 to 0.125
- convolution_signal_weight: bfloat16 [2048, 1024], P(None, 'tp'), may hold values from -0.125 to 0.125
- convolution_kernel_taps: bfloat16 [3, 1024], replicated, may hold values from -3.5 to 3.5
- memory_query_matrix: bfloat16 [2048, 512], P(None, 'tp'), may hold values from -0.125 to 0.125
- memory_key_matrix: bfloat16 [2048, 512], P(None, 'tp'), may hold values from -0.125 to 0.125
- memory_value_matrix: bfloat16 [2048, 1024], P(None, 'tp'), may hold values from -0.125 to 0.125
- output_gate_weight: bfloat16 [2048, 1024], P(None, 'tp'), may hold values from -0.125 to 0.125
- input_gate_weight: bfloat16 [2048, 8], replicated, may hold values from -0.5 to 0.5
- forget_gate_weight: bfloat16 [2048, 8], replicated, may hold values from -0.125 to 0.125
- input_gate_bias: float32 [8], replicated, may hold values from -1 to 125
- forget_gate_bias: float32 [8], replicated, may hold values from 3.5 to 12.5
- position_forget_factor: float32 [12288], P('sp'), may hold values from 0.5 to 2
- extra_log_decay: float32 [12288, 8], P('sp'), may hold values from -0.7 to 0
- starting_memory_state: float32 [8, 64, 128], replicated, may hold values from -6 to 6
- starting_log_scale: float32 [8], replicated, may hold values from 5 to 125
- head_norm_gain: bfloat16 [1024], replicated, may hold values from 0.099609375 to 1.8984375
- convolution_output_weight: bfloat16 [1024, 2048], P('tp'), may hold values from -0.125 to 0.125
- memory_output_weight: bfloat16 [1024, 2048], P('tp'), may hold values from -0.125 to 0.125
Outputs:
- mixed: bfloat16 [12288, 2048], P(('sp', 'tp'))
All inputs are finite; a program needn't handle non-finite values.
Results may differ from a plain program's by a relative error of at most 0.035.
Values may be sent and summed in bfloat16 or wider, within the bound.
A program may use at most 64 MiB of HBM per device.

v0:
```python
import jax
import jax.numpy as jnp
from jax import lax
from jax.sharding import PartitionSpec as P

DQK = 64
DV = 128
SPAN = 128


EPS = 1e-06
HIGHEST_PRECISION = lax.Precision.HIGHEST
FLOOR_LOG = -1e30


def from_behind(value, axis, by):
    devices = lax.axis_size(axis)
    pairs = [(i, i + by) for i in range(devices) if 0 <= i + by < devices]
    return lax.ppermute(value, axis, pairs)


def merge_states(earlier, later):
    state_one, peak_one, decay_one = earlier
    state_two, peak_two, decay_two = later
    lifted = peak_one + decay_two
    ceiling = jnp.maximum(lifted, peak_two)
    merged = (
        jnp.exp(lifted - ceiling)[..., None, None] * state_one
        + jnp.exp(peak_two - ceiling)[..., None, None] * state_two
    )
    return (merged, ceiling, decay_one + decay_two)


def block_terms(key_blocks, value_blocks, input_blocks, forget_blocks):
    cumulative = jnp.cumsum(forget_blocks, axis=2)
    block_total = cumulative[:, :, -1]
    weight_log = block_total[:, :, None] - cumulative + input_blocks
    block_peak = jnp.max(weight_log, axis=2)
    weights = jnp.exp(weight_log - block_peak[:, :, None])
    block_state = jnp.einsum(
        "nhld,nhle->nhde",
        key_blocks * weights[..., None],
        value_blocks,
        precision=HIGHEST_PRECISION,
    )
    return (cumulative, block_state, block_peak, block_total)


def block_outputs(
    query_blocks, key_blocks, value_blocks, input_blocks, cumulative, start_state, start_peak
):
    span_len = query_blocks.shape[2]
    carried = cumulative + start_peak[:, :, None]
    pair_log = cumulative[:, :, :, None] - cumulative[:, :, None, :] + input_blocks[:, :, None, :]
    causal = jnp.tril(jnp.ones((span_len, span_len), dtype=bool))
    pair_log = jnp.where(causal, pair_log, -jnp.inf)
    ceiling = jnp.maximum(carried, jnp.max(pair_log, axis=3))
    scores = jnp.einsum(
        "nhtd,nhsd->nhts", query_blocks, key_blocks, precision=HIGHEST_PRECISION
    ) * jnp.exp(pair_log - ceiling[..., None])
    local_part = jnp.einsum("nhts,nhse->nhte", scores, value_blocks, precision=HIGHEST_PRECISION)
    remote = jnp.einsum("nhtd,nhde->nhte", query_blocks, start_state, precision=HIGHEST_PRECISION)
    return jnp.exp(carried - ceiling)[..., None] * remote + local_part


def head_slice(source, piece_size, along):
    return lax.dynamic_slice_in_dim(source, lax.axis_index("tp") * piece_size, piece_size, along)


def on_device(
    tokens,
    input_norm_gain,
    convolution_outer_weight,
    convolution_inner_weight,
    convolution_signal_weight,
    convolution_kernel_taps,
    memory_query_matrix,
    memory_key_matrix,
    memory_value_matrix,
    output_gate_weight,
    input_gate_weight,
    forget_gate_weight,
    input_gate_bias,
    forget_gate_bias,
    position_forget_factor,
    extra_log_decay,
    starting_memory_state,
    starting_log_scale,
    head_norm_gain,
    convolution_output_weight,
    memory_output_weight,
):
    gathered = lax.all_gather(tokens, "tp", axis=0, tiled=True)
    row_count = gathered.shape[0]
    widened = gathered.astype(jnp.float32)
    normed = (
        widened
        * lax.rsqrt(jnp.mean(widened * widened, axis=1, keepdims=True) + EPS)
        * input_norm_gain.astype(jnp.float32)
    ).astype(jnp.bfloat16)

    def project(weight):
        return jnp.dot(normed, weight, preferred_element_type=jnp.float32).astype(jnp.bfloat16)

    outer_gate = project(convolution_outer_weight)
    inner_gate = project(convolution_inner_weight)
    signal = project(convolution_signal_weight)
    channels = convolution_outer_weight.shape[1]
    conv_reach = convolution_kernel_taps.shape[0] - 1
    rim_rows = jnp.stack([inner_gate[row_count - conv_reach :], signal[row_count - conv_reach :]])
    before_rows = from_behind(rim_rows, "sp", 1)
    full_inner = jnp.concatenate([before_rows[0], inner_gate], axis=0).astype(jnp.float32)
    full_signal = jnp.concatenate([before_rows[1], signal], axis=0).astype(jnp.float32)
    mixed_in = full_inner * full_signal
    tap_weights = head_slice(convolution_kernel_taps, channels, 1).astype(jnp.float32)
    conv_sum = jnp.zeros((row_count, channels), jnp.float32)
    for offset in range(conv_reach + 1):
        conv_sum = conv_sum + tap_weights[offset] * mixed_in[offset : offset + row_count]
    conv_out = (outer_gate.astype(jnp.float32) * conv_sum).astype(jnp.bfloat16)
    head_count = memory_query_matrix.shape[1] // DQK
    queries = project(memory_query_matrix)
    key_rows = project(memory_key_matrix)
    value_rows = project(memory_value_matrix)
    out_gate = project(output_gate_weight)
    input_all = (
        jnp.dot(normed, input_gate_weight, preferred_element_type=jnp.float32) + input_gate_bias
    )
    forget_gate_values = (
        jnp.dot(normed, forget_gate_weight, preferred_element_type=jnp.float32) + forget_gate_bias
    )
    forget_gate_logs = (
        position_forget_factor[:, None] * jax.nn.log_sigmoid(forget_gate_values) + extra_log_decay
    )
    log_input = head_slice(input_all, head_count, 1)
    forget_log_values = head_slice(forget_gate_logs, head_count, 1)
    block_count = row_count // SPAN

    def heads_first(source, column_width):
        return (
            source.astype(jnp.float32)
            .reshape(block_count, SPAN, head_count, column_width)
            .transpose(0, 2, 1, 3)
        )

    def gates_first(source):
        return source.reshape(block_count, SPAN, head_count).transpose(0, 2, 1)

    query_blocks = heads_first(queries, DQK) * DQK ** (-0.5)
    key_blocks = heads_first(key_rows, DQK)
    value_blocks = heads_first(value_rows, DV)
    input_blocks = gates_first(log_input)
    forget_blocks = gates_first(forget_log_values)
    cumulative, block_state, block_peak, block_total = block_terms(
        key_blocks, value_blocks, input_blocks, forget_blocks
    )
    identity = (
        jnp.zeros((head_count, DQK, DV), jnp.float32),
        jnp.full((head_count,), FLOOR_LOG, jnp.float32),
        jnp.zeros((head_count,), jnp.float32),
    )

    def advance(carried_state, block_item):
        return (merge_states(carried_state, block_item), carried_state)

    device_sum, within = lax.scan(advance, identity, (block_state, block_peak, block_total))
    decay_rows = lax.all_gather(device_sum[2][None], "sp", axis=0, tiled=True)
    cumul_ends = jnp.cumsum(decay_rows, axis=0)
    my_index = lax.axis_index("sp")
    before_decay = lax.dynamic_index_in_dim(cumul_ends, my_index, 0, keepdims=False) - device_sum[2]
    piece_state = lax.all_gather(device_sum[0][None], "sp", axis=0, tiled=True)
    piece_peak = lax.all_gather(device_sum[1][None], "sp", axis=0, tiled=True)
    piece_count = piece_peak.shape[0]
    position = jnp.arange(piece_count, dtype=jnp.int32)
    earlier_mask = (position < my_index)[:, None]
    scale_log = jnp.where(earlier_mask, piece_peak - cumul_ends, FLOOR_LOG)
    ceiling = jnp.maximum((identity[0], identity[1])[1], jnp.max(scale_log, axis=0))
    factor = jnp.where(earlier_mask, jnp.exp(scale_log - ceiling), 0.0)
    merged = jnp.einsum("ph,phde->hde", factor, piece_state, precision=HIGHEST_PRECISION)
    before_me = (merged, ceiling + before_decay, before_decay)
    own_initial = (
        head_slice(starting_memory_state, head_count, 0),
        head_slice(starting_log_scale, head_count, 0),
        jnp.zeros((head_count,), jnp.float32),
    )
    start_zero = merge_states(own_initial, before_me)
    block_starts = merge_states(
        (start_zero[0][None], start_zero[1][None], start_zero[2][None]), within
    )
    numerator = block_outputs(
        query_blocks,
        key_blocks,
        value_blocks,
        input_blocks,
        cumulative,
        block_starts[0],
        block_starts[1],
    )
    numerator = numerator.transpose(0, 2, 1, 3).reshape(row_count, head_count, DV)
    normal_rows = numerator * lax.rsqrt(
        jnp.mean(numerator * numerator, axis=2, keepdims=True) + EPS
    )
    own_gain = head_slice(head_norm_gain, head_count * DV, 0).astype(jnp.float32)
    memory_out = (
        normal_rows.reshape(row_count, head_count * DV)
        * own_gain
        * jax.nn.sigmoid(out_gate.astype(jnp.float32))
    ).astype(jnp.bfloat16)
    return lax.psum_scatter(
        (
            jnp.dot(conv_out, convolution_output_weight, preferred_element_type=jnp.float32)
            + jnp.dot(memory_out, memory_output_weight, preferred_element_type=jnp.float32)
        ).astype(jnp.bfloat16),
        "tp",
        scatter_dimension=0,
        tiled=True,
    )


def solution(mesh):
    in_specs = (
        P(("sp", "tp"), None),
        P(),
        P(None, "tp"),
        P(None, "tp"),
        P(None, "tp"),
        P(),
        P(None, "tp"),
        P(None, "tp"),
        P(None, "tp"),
        P(None, "tp"),
        P(),
        P(),
        P(),
        P(),
        P("sp"),
        P("sp", None),
        P(),
        P(),
        P(),
        P("tp", None),
        P("tp", None),
    )
    out_specs = P(("sp", "tp"), None)
    return jax.shard_map(
        on_device, mesh=mesh, in_specs=in_specs, out_specs=out_specs, check_vma=False
    )
```

profile of v0, /device:TPU:0, one launch (start us, length us, event | category | flops | bytes accessed | tf_op | source)
XLA Modules:
  0.0 271.6 jit_solution(17865871519124520176)
XLA Ops:
  8.1 1.2 dynamic-slice
  11.2 1.3 dynamic-slice_convert_fusion.1
  14.4 42.1 %all-gather.6.cloned.1.call-done = bf16[768,2048]{1,0:T(8,128)(2,1)} async-done(((bf16[384,2048]{1,0:T(8,128)(2,1)}), bf16[768,2048]{1,0:T(8,128)(2,1)}) %all-gather.6.cloned.1.call-update) | async-done | bytes 3145744 | tf_op jit(solution)/shard_map/all_gather | solution.py:93
  56.5 2.7 %fusion.8 = f32[768]{0:T(1024)S(1)} fusion(bf16[768,2048]{1,0:T(8,128)(2,1)} %all-gather.6.cloned.1.call-done), kind=kLoop, calls=%fused_computation.18 | loop fusion | flops 4717824 | bytes 3148800 | tf_op jit(solution)/shard_map/reduce_sum | solution.py:98
  61.9 0.9 negate_exponential_fusion
  62.9 1.8 reduce_window_sum.22
  65.9 3.1 %convolution_convert_fusion.6 = bf16[768,256]{1,0:T(8,128)(2,1)S(1)} fusion(bf16[768,2048]{1,0:T(8,128)(2,1)} %copy-done.1, bf16[2048,256]{1,0:T(8,128)(2,1)} %param.30), kind=kOutput, calls=%fused_computation.53 | convolution fusion | flops 805502976 | bytes 4587520 | tf_op jit(solution)/shard_map/dot_general | solution.py:103
  69.7 4.5 %convolution_convert_fusion.2 = bf16[768,512]{1,0:T(8,128)(2,1)S(1)} fusion(bf16[768,2048]{1,0:T(8,128)(2,1)} %copy-done.1, bf16[2048,512]{1,0:T(8,128)(2,1)} %param.27), kind=kOutput, calls=%fused_computation.47 | convolution fusion | flops 1611005952 | bytes 6029312 | tf_op jit(solution)/shard_map/dot_general | solution.py:103
  74.2 1.8 convolution_convert_fusion.3
  77.5 2.2 collective-permute-start
  79.7 1.8 convolution_convert_fusion.1
  81.5 1.1 reshape.88
  82.5 1.5 copy.72
  84.8 2.5 fusion.30
  87.3 47.3 %while.21 = (s32[]{:T(128)}, f32[4,64,128]{2,1,0:T(8,128)S(1)}, f32[4]{0:T(128)}, f32[4]{0:T(128)}, f32[6,4,64,128]{3,2,1,0:T(8,128)}, /*index=5*/f32[6,4]{1,0:T...) while((s32[]{:T(128)}, f32[4,64,128]{2,1,0:T(8,128)S(1)}, ...), condition=%wide.region_4.5_spmd.clone, body=%wide.region_3.4_spmd.clone.sunk | while | flops 163875 | bytes 655826 | solution.py:165
  87.9 1.3 subtract_exponential_fusion.9
  89.2 1.2 subtract_exponential_fusion.10
  90.4 1.3 dynamic_update_slice.20
  91.7 1.3 dynamic_update_slice.19
  93.6 1.0 fusion.96
  94.7 1.3 fusion.97
  95.9 1.3 subtract_exponential_fusion.9
  97.2 1.2 subtract_exponential_fusion.10
  98.4 1.3 dynamic_update_slice.20
  99.7 1.3 dynamic_update_slice.19
  101.6 1.0 fusion.96
  102.7 1.3 fusion.97
  103.9 1.3 subtract_exponential_fusion.9
  105.2 1.2 subtract_exponential_fusion.10
  106.4 1.3 dynamic_update_slice.20
  107.7 1.3 dynamic_update_slice.19
  109.6 1.0 fusion.96
  110.7 1.3 fusion.97
  111.9 1.3 subtract_exponential_fusion.9
  113.2 1.2 subtract_exponential_fusion.10
  114.4 1.3 dynamic_update_slice.20
  115.7 1.3 dynamic_update_slice.19
  117.6 1.0 fusion.96
  118.7 1.3 fusion.97
  119.9 1.3 subtract_exponential_fusion.9
  121.2 1.2 subtract_exponential_fusion.10
  122.4 1.3 dynamic_update_slice.20
  123.7 1.3 dynamic_update_slice.19
  125.6 1.0 fusion.96
  126.6 1.3 fusion.97
  127.9 1.3 subtract_exponential_fusion.9
  129.2 1.2 subtract_exponential_fusion.10
  130.4 1.3 dynamic_update_slice.20
  131.7 1.3 dynamic_update_slice.19
  133.6 1.0 fusion.96
  135.4 4.0 %fusion.26 = f32[768,256]{1,0:T(8,128)} fusion(bf16[768,2048]{1,0:T(8,128)(2,1)} %copy-done.1, bf16[2048,256]{1,0:T(8,128)(2,1)} %param.29), kind=kOutput, calls=%fused_computation.52 | convolution fusion | flops 805896192 | bytes 4980736 | tf_op jit(solution)/shard_map/dot_general | solution.py:103
  139.5 2.3 copy.61
  141.8 2.2 mul.209
  144.4 32.5 %all-reduce.2 = (f32[64]{0:T(128)S(1)}, f32[64]{0:T(128)S(1)}) all-reduce(f32[64]{0:T(128)S(1)} %dynamic-update-slice, f32[64]{0:T(128)S(1)} %dynamic-update-slice.1), channel_id=2, replica_groups=mesh['sp'=16,'tp'=2] {'sp'}, use_global_device_ids=true, to_apply=%add | all-reduce | flops 128 | bytes 1024
  180.2 2.6 fusion.45
  182.9 3.4 %fusion.20 = f32[6,4,128,128]{2,3,1,0:T(8,128)} fusion(f32[6,4,128,128]{3,2,1,0:T(8,128)S(1)} %fusion.45, bf16[6,128,4,128]{1,3,2,0:T(8,128)(2,1)S(1)} %copy.72, f32[6,4,128]{2,1,0:T(4,128)S(1)} %add_maximum_fusion, f32[6,4,128]{2,1,0:T(4,128)S(1)} %copy-done.10, f32[6,4,128]{2,1,0:T(4,128)S(1)} %reduce_window_sum.22, pred[128,128]{1,0:T(8,128)(4,1)S(1)} %copy-done.11), kind=kOutput, calls=%fused_computation.39 | convolution fusion | flops 605945856 | bytes 3985408 | tf_op jit(solution)/shard_map/nhts,nhse->nhte/dot_general | solution.py:61
  187.0 3.0 %convert_multiply_fusion.2 = f32[770,512]{1,0:T(8,128)} fusion(bf16[768,512]{1,0:T(8,128)(2,1)} %copy-done.8, bf16[2,512]{1,0:T(2,128)(2,1)S(1)} %get-tuple-element.178, bf16[768,512]{1,0:T(8,128)(2,1)} %copy-done.7, bf16[2,512]{1,0:T(2,128)(2,1)S(1)} %get-tuple-element.177), kind=kLoop, calls=%fused_computation.24 | loop fusion | flops 3548160 | bytes 3153920 | tf_op jit(solution)/shard_map/mul | solution.py:114
  190.0 10.3 %fusion.28 = f32[768,2048]{1,0:T(8,128)} fusion(bf16[512,2048]{1,0:T(8,128)(2,1)S(1)} %copy-done, f32[770,512]{1,0:T(8,128)} %convert_multiply_fusion.2, bf16[768,2048]{1,0:T(8,128)(2,1)} %copy-done.1, bf16[2048,512]{1,0:T(8,128)(2,1)} %param.25, f32[512]{0:T(512)S(1)} %bitcast.143, f32[512]{0:T(512)S(1)} %bitcast.144, f32[512]{0:T(512)S(1)} %bitcast.142), kind=kOutput, calls=%fused_computation.57 | convolution fusion | flops 3224764416 | bytes 18356224 | tf_op jit(solution)/shard_map/dot_general | solution.py:210
  200.4 3.9 %fusion.11 = f32[4,1,64,128]{3,1,2,0:T(1,128)S(1)} fusion(f32[16,4,1,1]{0,2,3,1:T(1,128)S(1)} %copy.68, f32[16,4,64,128]{3,2,1,0:T(8,128)} %bitcast.137), kind=kOutput, calls=%fused_computation.22 | convolution fusion | flops 6291456 | bytes 2228480 | tf_op jit(solution)/shard_map/ph,phde->hde/dot_general | solution.py:178
  204.5 5.0 %multiply_reduce_fusion = (f32[6,128,4]{1,2,0:T(4,128)S(1)}, f32[6,128,4,128]{1,3,2,0:T(8,128)}) fusion(f32[6,4,128,128]{2,3,1,0:T(8,128)S(1)} %copy-done.6, f32[6,4,64,128]{3,2,1,0:T(8,128)} %get-tuple-element.67, f32[6,4]{1,0:T(8,128)S(1)} %subtract_exponential_fusion.3, f32[4,64,128]{2,1,0:T(8,128)S(1)} %multiply_add_fusion, ...), kind=kOutput, calls=%fused_computation.38 | convolution fusion | flops 304149504 | bytes 4874432 | tf_op jit(solution)/shard_map/nhtd,nhde->nhte/dot_general | solution.py:62
  209.8 2.6 copy.65
  212.3 1.8 mul.223
  214.2 11.1 %add_convert_fusion = bf16[768,2048]{1,0:T(8,128)(2,1)} fusion(f32[768,2048]{1,0:T(8,128)} %fusion.28, bf16[512,2048]{1,0:T(8,128)(2,1)} %param.43, f32[96,8,4,128]{3,2,1,0:T(4,128)} %bitcast.139, f32[96,8,4,128]{3,2,1,0:T(4,128)} %bitcast.138, bf16[768,2048]{1,0:T(8,128)(2,1)} %copy-done.1, bf16[2048,512]{1,0:T(8,128)(2,1)} %param.32, f32[512]{0:T(512)S(1)} %copy-done.27), kind=kOutput, calls=%fused_computation.21 | convolution fusion | flops 3227910144 | bytes 19924992 | tf_op jit(solution)/shard_map/dot_general | solution.py:211
  225.3 39.8 %reduce-scatter.2.cloned.1.call-done = bf16[384,2048]{1,0:T(8,128)(2,1)} async-done(((bf16[768,2048]{1,0:T(8,128)(2,1)}), bf16[384,2048]{1,0:T(8,128)(2,1)}) %reduce-scatter.2.cloned.1.call-update) | async-done | bytes 1572880 | tf_op jit(solution)/shard_map/reduce_scatter | solution.py:208
  (131 shorter events, 21.4 us)
Async XLA Ops:
  6.5 183.5 %copy-start = (bf16[512,2048]{1,0:T(8,128)(2,1)S(1)}, bf16[512,2048]{1,0:T(8,128)(2,1)}, u32[]{:S(2)}) copy-start(bf16[512,2048]{1,0:T(8,128)(2,1)} %param.42) | copy-start | bytes 6291460
  6.5 50.0 %all-gather.6.cloned.1.call-start = ((), (), s32[]{:S(2)}) async-start(), calls=%async_computation.1 | async-start | bytes 4718592 | tf_op jit(solution)/shard_map/all_gather | solution.py:93
  7.3 193.1 %all-gather.8.cloned.1.call-start = ((), (), s32[]{:S(2)}) async-start(), calls=%async_computation.3 | async-start | bytes 2228224 | tf_op jit(solution)/shard_map/all_gather | solution.py:170
  56.5 2.8 %copy-start.4 = (bf16[768,2048]{1,0:T(8,128)(2,1)S(1)}, bf16[768,2048]{1,0:T(8,128)(2,1)}, u32[]{:S(2)}) copy-start(bf16[768,2048]{1,0:T(8,128)(2,1)} %all-gather.6.cloned.1.call-done) | copy-start | bytes 9437188
  59.4 0.8 copy-start.17
  60.2 1.7 copy-start.1
  60.2 1.7 copy-start.16
  60.2 1.7 copy-start.23
  61.9 1.0 copy-start.20
  61.9 1.0 copy-start.22
  65.2 0.7 copy-start.9
  65.2 0.7 copy-start.15
  69.7 4.5 %copy-start.2 = (bf16[768,2048]{1,0:T(8,128)(2,1)S(1)}, bf16[768,2048]{1,0:T(8,128)(2,1)}, u32[]{:S(2)}) copy-start(bf16[768,2048]{1,0:T(8,128)(2,1)} %copy-done.1) | copy-start | bytes 9437188
  69.7 4.5 %copy-start.32 = (bf16[2048,512]{1,0:T(8,128)(2,1)S(1)}, bf16[2048,512]{1,0:T(8,128)(2,1)}, u32[]{:S(2)}) copy-start(bf16[2048,512]{1,0:T(8,128)(2,1)} %param.26) | copy-start | bytes 6291460
  74.2 1.8 copy-start.7
  74.2 5.5 %copy-start.33 = (bf16[2048,512]{1,0:T(8,128)(2,1)S(1)}, bf16[2048,512]{1,0:T(8,128)(2,1)}, u32[]{:S(2)}) copy-start(bf16[2048,512]{1,0:T(8,128)(2,1)} %param.31) | copy-start | bytes 6291460
  76.0 0.9 copy-start.8
  77.5 108.8 %collective-permute-start = (bf16[2,2,512]{2,1,0:T(2,128)(2,1)}, bf16[2,2,512]{2,1,0:T(2,128)(2,1)}, u32[]{:S(2)}, u32[]{:S(2)}) collective-permute-start(bf16[2,2,512]{2,1,0:T(2,128)(2,1)} %pad_maximum_fusion), channel_id=1, source_target_pairs={{0,2},{2,4},{4,6},{6,8},{8,10},{10,12},{12,14},{14,16},{16,18},{18... | collective-permute-start | bytes 12296 | tf_op jit(solution)/shard_map/ppermute | solution.py:19
  134.6 0.7 copy-start.3
  135.3 129.8 %reduce-scatter.2.cloned.1.call-start = ((), (), s32[]{:S(2)}) async-start(), calls=%async_computation.2 | async-start | bytes 4718592 | tf_op jit(solution)/shard_map/reduce_scatter | solution.py:208
  139.4 4.6 %copy-start.18 = (f32[4]{0:T(128)S(1)}, f32[4]{0:T(128)}, u32[]{:S(2)}) copy-start(f32[4]{0:T(128)} %get-tuple-element.62) | copy-start | bytes 52
  139.4 4.8 %copy-start.13 = (f32[4]{0:T(128)S(1)}, f32[4]{0:T(128)}, u32[]{:S(2)}) copy-start(f32[4]{0:T(128)} %get-tuple-element.63) | copy-start | bytes 52
  139.4 37.8 %copy-start.26 = (pred[16]{0:T(512)(128)(4,1)S(1)}, pred[16]{0:T(512)(128)(4,1)}, u32[]{:S(2)}) copy-start(pred[16]{0:T(512)(128)(4,1)} %iota_compare_fusion.1) | copy-start | bytes 52
  139.4 37.9 %copy-start.10 = (f32[6,4,128]{2,1,0:T(4,128)S(1)}, f32[6,4,128]{2,1,0:T(4,128)}, u32[]{:S(2)}) copy-start(f32[6,4,128]{2,1,0:T(4,128)} %copy-done.9) | copy-start | bytes 36868
  139.4 37.9 %copy-start.11 = (pred[128,128]{1,0:T(8,128)(4,1)S(1)}, pred[128,128]{1,0:T(8,128)(4,1)}, u32[]{:S(2)}) copy-start(pred[128,128]{1,0:T(8,128)(4,1)} %iota_compare_fusion) | copy-start | bytes 49156
  139.4 38.8 %copy-start.31 = (f32[8]{0:T(128)S(1)}, f32[8]{0:T(128)}, u32[]{:S(2)}) copy-start(f32[8]{0:T(128)} %param.40) | copy-start | bytes 100
  139.4 39.9 %copy-start.19 = (f32[6,4]{1,0:T(8,128)S(1)}, f32[6,4]{1,0:T(8,128)}, u32[]{:S(2)}) copy-start(f32[6,4]{1,0:T(8,128)} %get-tuple-element.65) | copy-start | bytes 292
  139.4 39.9 %copy-start.21 = (f32[6,4]{1,0:T(8,128)S(1)}, f32[6,4]{1,0:T(8,128)}, u32[]{:S(2)}) copy-start(f32[6,4]{1,0:T(8,128)} %get-tuple-element.64) | copy-start | bytes 292
  186.2 3.8 %copy-start.28 = (f32[1,512]{1,0:T(1,128)S(1)}, f32[1,512]{1,0:T(1,128)}, u32[]{:S(2)}) copy-start(f32[1,512]{1,0:T(1,128)} %get-tuple-element.174) | copy-start | bytes 6148
  186.2 3.8 %copy-start.29 = (f32[1,512]{1,0:T(1,128)S(1)}, f32[1,512]{1,0:T(1,128)}, u32[]{:S(2)}) copy-start(f32[1,512]{1,0:T(1,128)} %get-tuple-element.175) | copy-start | bytes 6148
  186.2 3.8 %copy-start.30 = (f32[1,512]{1,0:T(1,128)S(1)}, f32[1,512]{1,0:T(1,128)}, u32[]{:S(2)}) copy-start(f32[1,512]{1,0:T(1,128)} %get-tuple-element.176) | copy-start | bytes 6148
  190.0 14.3 %copy-start.12 = (f32[8,64,128]{2,1,0:T(8,128)S(1)}, f32[8,64,128]{2,1,0:T(8,128)}, u32[]{:S(2)}) copy-start(f32[8,64,128]{2,1,0:T(8,128)} %param.39) | copy-start | bytes 786436
  200.4 4.0 %copy-start.24 = (f32[4]{0:T(128)S(1)}, f32[4]{0:T(128)}, u32[]{:S(2)}) copy-start(f32[4]{0:T(128)} %get-tuple-element.167) | copy-start | bytes 52
  200.4 4.0 %copy-start.25 = (f32[4]{0:T(128)S(1)}, f32[4]{0:T(128)}, u32[]{:S(2)}) copy-start(f32[4]{0:T(128)} %get-tuple-element.179) | copy-start | bytes 52
  200.4 4.1 %copy-start.5 = (f32[6,128,4,64]{1,0,3,2:T(8,128)S(1)}, f32[6,128,4,64]{1,0,3,2:T(8,128)}, u32[]{:S(2)}) copy-start(f32[6,128,4,64]{1,0,3,2:T(8,128)} %mul.209) | copy-start | bytes 2359300
  200.4 4.1 %copy-start.14 = (f32[6,128,4]{1,2,0:T(4,128)S(1)}, f32[6,128,4]{1,2,0:T(4,128)}, u32[]{:S(2)}) copy-start(f32[6,128,4]{1,2,0:T(4,128)} %fusion.52) | copy-start | bytes 36868
  200.4 4.1 %copy-start.6 = (f32[6,4,128,128]{2,3,1,0:T(8,128)S(1)}, f32[6,4,128,128]{2,3,1,0:T(8,128)}, u32[]{:S(2)}) copy-start(f32[6,4,128,128]{2,3,1,0:T(8,128)} %fusion.20) | copy-start | bytes 4718596
  209.7 4.4 %copy-start.27 = (f32[512]{0:T(512)S(1)}, f32[512]{0:T(512)}, u32[]{:S(2)}) copy-start(f32[512]{0:T(512)} %dynamic-slice_convert_fusion.1) | copy-start | bytes 6148
Sparse Core Ops, SparseCore 0:
  8.9 47.6 all-gather.5
  135.4 41.8 all-gather.7
  225.4 39.6 reduce-scatter.1
where the time goes:
time: 273 us; the launch traced here: 272 us
  waiting for transfers between devices  82.7 us (30%)
  matrix products  56 us (21%)
  other arithmetic  48.7 us (18%)
  local copies, waits for them, and re-layouts  35 us (13%)
  blocking collectives  32.5 us (12%)
  between operations  14.3 us (5%)
    all_gather x1, waiting for transfers between devices, on_device(): gathered = lax.all_gather(tokens, 'tp', axis=0, tiled=True)  42.1 us
    reduce_scatter x1, waiting for transfers between devices, on_device(): lax.psum_scatter((jnp.dot(conv_out, convolution_output_weight, preferred_...  39.8 us
    unnamed x1, blocking collectives  32.5 us
    dynamic_update_slice x12, local copies, waits for them, and re-layouts, on_device(): lax.scan(advance, identity, (block_state, block_peak, block_total))  15.4 us
    dot_general x5, matrix products, project(): jnp.dot(normed, weight, preferred_element_type=jnp.float32)  15.2 us
    dot_general x1, matrix products, on_device(): jnp.dot(memory_out, memory_output_weight, preferred_element_type=jnp.floa...  11.1 us
    dot_general x1, matrix products, on_device(): jnp.dot(conv_out, convolution_output_weight, preferred_element_type=jnp.f...  10.3 us
    exp x8, other arithmetic, merge_states(): jnp.exp(lifted - ceiling)[..., None, None] * state_one  8.29 us
  transfers between devices with their start and end apart: 4, of which 2 were waited for; matrix products, arithmetic and copies ran while one was open for 34% of the time, Pallas kernels for 0%

commit v1 on v0

v1 whole, which is shorter than its diff:
```python
import functools

import jax
import jax.numpy as jnp
from jax import lax
from jax.experimental import pallas as pl
from jax.experimental.pallas import tpu as pltpu
from jax.sharding import PartitionSpec as P

DQK = 64
DV = 128
EPS = 1e-06
FLOOR_LOG = -1e30
MESH = pl.DeviceIdType.MESH
BF = jnp.bfloat16
F32 = jnp.float32


def scan_lanes(x, op, fill):
    width = x.shape[1]
    lane = lax.broadcasted_iota(jnp.int32, x.shape, 1)
    shift = 1
    while shift < width:
        x = op(x, jnp.where(lane >= shift, pltpu.roll(x, shift, 1), fill))
        shift *= 2
    return x


def merge(earlier, later):
    s1, p1, d1 = earlier
    s2, p2, d2 = later
    lifted = p1 + d2
    top = jnp.maximum(lifted, p2)
    w1 = jnp.exp(lifted - top)
    w2 = jnp.exp(p2 - top)
    return ([w1[h : h + 1] * s1[h] + w2[h : h + 1] * s2[h] for h in range(len(s1))], top, d1 + d2)


def kernel(
    n_sp, n_tp,
    tok, gain, wo, wi, ws, taps, wq, wk, wv, wg, gin, gfo, bin_, bfo, pos, extra, s0, p0, hgain, wco, wmo,
    out,
    rows, vo, vi, vs, vq, vk, vv, vg, vco, vmo,
    ao, mix, aq, ak, av, ag, gates, gates_t, own_t, own_c, local, halo_send,
    st_send, st_recv, sc_send, sc_recv, start_s, start_p, part_send, part_recv,
    wsem, tsend, trecv, hsem, ssend, srecv, psend, precv,
):
    me = lax.axis_index("tp")
    sq = lax.axis_index("sp")
    own = tok.shape[0]
    total = rows.shape[0]
    ch = 128 if own % 128 == 0 else own
    nch = own // ch
    heads = aq.shape[1] // DQK
    mh = gin.shape[1]
    cw = ao.shape[1]
    rounds = n_sp.bit_length() - 1

    pairs = [(wo, vo), (wi, vi), (ws, vs), (wq, vq), (wk, vk), (wv, vv), (wg, vg), (wco, vco), (wmo, vmo)]
    loads = [pltpu.make_async_copy(src, dst, wsem.at[i]) for i, (src, dst) in enumerate(pairs)]
    for load in loads:
        load.start()

    def partner(r):
        bit = (sq // (1 << r)) % 2
        return bit, sq + (1 - 2 * bit) * (1 << r)

    barrier = pltpu.get_barrier_semaphore()
    for k in range(1, n_tp):
        pl.semaphore_signal(barrier, inc=1, device_id={"tp": lax.rem(me + k, n_tp)}, device_id_type=MESH)
    for r in range(rounds):
        pl.semaphore_signal(barrier, inc=1, device_id={"sp": partner(r)[1]}, device_id_type=MESH)
    pl.semaphore_signal(barrier, inc=1, device_id={"sp": lax.rem(sq + 1, n_sp)}, device_id_type=MESH)
    pl.semaphore_signal(barrier, inc=1, device_id={"sp": lax.rem(sq + n_sp - 1, n_sp)}, device_id_type=MESH)
    pl.semaphore_wait(barrier, n_tp - 1 + rounds + 2)

    def token_copy(k, c):
        return pltpu.make_async_remote_copy(
            src_ref=tok.at[pl.ds(c * ch, ch)],
            dst_ref=rows.at[pl.ds(pl.multiple_of(me * own + c * ch, 8), ch)],
            send_sem=tsend.at[k - 1, c],
            recv_sem=trecv.at[n_tp - k - 1, c],
            device_id={"tp": lax.rem(me + k, n_tp)},
            device_id_type=MESH,
        )

    sends = [token_copy(k, c) for c in range(nch) for k in range(1, n_tp)]
    for copy in sends:
        copy.start()
    rows[pl.ds(pl.multiple_of(me * own, 8), own), :] = tok[...]
    for load in loads:
        load.wait()
    gates[...] = jnp.zeros_like(gates)
    own_t[...] = jnp.zeros_like(own_t)

    def project(step, carry):
        k = step // nch
        c = step % nch
        owner = lax.rem(me + k, n_tp)
        r0 = pl.multiple_of(owner * own + c * ch, 8)
        spot = pl.ds(r0, ch)

        @pl.when(step >= nch)
        def _():
            pltpu.make_async_remote_copy(
                src_ref=tok.at[pl.ds(0, ch)],
                dst_ref=rows.at[spot],
                send_sem=tsend.at[0, 0],
                recv_sem=trecv.at[k - 1, c],
                device_id={"tp": owner},
                device_id_type=MESH,
            ).wait_recv()

        wide = rows[spot, :].astype(F32)
        scale = lax.rsqrt(jnp.mean(wide * wide, axis=1, keepdims=True) + EPS)
        normed = (wide * scale * gain[...].astype(F32)).astype(BF)

        def dot(w):
            return jnp.dot(normed, w[...], preferred_element_type=F32)

        gates[spot, 0:mh] = dot(gfo) + bfo[...]
        gates[spot, mh : 2 * mh] = dot(gin) + bin_[...]
        gates[spot, 2 * mh : 3 * mh] = extra[spot, :]
        gates[spot, 3 * mh : 4 * mh] = jnp.broadcast_to(p0[...], (ch, mh))
        aq[spot, :] = (dot(vq) * DQK ** -0.5).astype(BF)
        ak[spot, :] = dot(vk).astype(BF)
        av[spot, :] = dot(vv).astype(BF)
        ag[spot, :] = dot(vg).astype(BF)
        ao[spot, :] = dot(vo).astype(BF)
        inner = dot(vi).astype(BF).astype(F32)
        signal = dot(vs).astype(BF).astype(F32)
        mix[pl.ds(r0 + 8, ch), :] = inner * signal
        return carry

    lax.fori_loop(0, n_tp * nch, project, 0)
    for copy in sends:
        copy.wait_send()

    halo_send[...] = mix[total : total + 8, :]
    halo_copy = pltpu.make_async_remote_copy(
        src_ref=halo_send,
        dst_ref=mix.at[pl.ds(0, 8)],
        send_sem=hsem.at[0],
        recv_sem=hsem.at[1],
        device_id={"sp": lax.rem(sq + 1, n_sp)},
        device_id_type=MESH,
    )
    halo_copy.start()

    gates_t[...] = gates[...].T

    def own_rows(group):
        picked = [gates_t[pl.ds(group * mh + me * heads + h, 1), :] for h in range(heads)]
        picked += [jnp.zeros((8 - heads, total), F32)] if heads < 8 else []
        return jnp.concatenate(picked, axis=0)

    pre = own_rows(0)
    log_sig = jnp.minimum(pre, 0.0) - jnp.log1p(jnp.exp(-jnp.abs(pre)))
    log_forget = pos[...] * log_sig + own_rows(2)
    cumul = scan_lanes(log_forget, jnp.add, 0.0)
    lifted_in = own_rows(1) - cumul
    running = scan_lanes(lifted_in, jnp.maximum, FLOOR_LOG)
    own_t[0:8, :] = lifted_in
    own_t[8:16, :] = running
    own_c[...] = own_t[...].T
    last_peak = jnp.broadcast_to(running[:, total - 1 : total], (8, DV))
    last_decay = jnp.broadcast_to(cumul[:, total - 1 : total], (8, DV))

    states = []
    for h in range(heads):
        weight = jnp.exp(own_c[:, h : h + 1] - last_peak[h : h + 1, 0:1])
        keyed = (ak[:, h * DQK : (h + 1) * DQK].astype(F32) * weight).astype(BF)
        states.append(
            lax.dot_general(keyed, av[:, h * DV : (h + 1) * DV], (((0,), (0,)), ((), ())), preferred_element_type=F32)
        )
    mine = (states, last_decay + last_peak, last_decay)
    before = (
        [jnp.zeros((DQK, DV), F32) for _ in range(heads)],
        jnp.full((8, DV), FLOOR_LOG, F32),
        jnp.zeros((8, DV), F32),
    )

    tile = 256

    def local_part(h):
        qh = aq[:, h * DQK : (h + 1) * DQK]
        kh = ak[:, h * DQK : (h + 1) * DQK]
        for t in range(total // tile):
            lo, end = t * tile, (t + 1) * tile
            scores = lax.dot_general(
                qh[lo:end], kh[:end], (((1,), (1,)), ((), ())), preferred_element_type=F32
            )
            gap = own_t[h : h + 1, 0:end] - own_c[lo:end, 8 + h : 9 + h]
            row = lax.broadcasted_iota(jnp.int32, (tile, end), 0) + lo
            col = lax.broadcasted_iota(jnp.int32, (tile, end), 1)
            weighted = (scores * jnp.exp(jnp.where(col <= row, gap, FLOOR_LOG))).astype(BF)
            local[lo:end, h * DV : (h + 1) * DV] = jnp.dot(
                weighted, av[0:end, h * DV : (h + 1) * DV], preferred_element_type=F32
            )

    done = 0
    for r in range(rounds):
        bit, other = partner(r)
        for h in range(heads):
            st_send[r, h] = mine[0][h].astype(BF)
        sc_send[r, 0:8] = mine[1]
        sc_send[r, 8:16] = mine[2]
        copies = [
            pltpu.make_async_remote_copy(
                src_ref=src.at[r], dst_ref=dst.at[r], send_sem=ssend.at[r, i], recv_sem=srecv.at[r, i],
                device_id={"sp": other}, device_id_type=MESH,
            )
            for i, (src, dst) in enumerate(((st_send, st_recv), (sc_send, sc_recv)))
        ]
        for copy in copies:
            copy.start()
        want = heads if r == rounds - 1 else -(-heads * (r + 1) // rounds)
        while done < want:
            local_part(done)
            done += 1
        for copy in copies:
            copy.wait()
        theirs = ([st_recv[r, h].astype(F32) for h in range(heads)], sc_recv[r, 0:8], sc_recv[r, 8:16])
        later = bit == 1

        def pick(a, b):
            return ([jnp.where(later, x, y) for x, y in zip(a[0], b[0])], jnp.where(later, a[1], b[1]), jnp.where(later, a[2], b[2]))

        before = pick(merge(theirs, before), before)
        if r < rounds - 1:
            mine = merge(pick(theirs, mine), pick(mine, theirs))

    first = (
        [s0[me * heads + h] for h in range(heads)],
        own_rows(3)[:, 0:DV],
        jnp.zeros((8, DV), F32),
    )
    start = merge(first, before)
    for h in range(heads):
        start_s[h] = start[0][h].astype(BF)
    start_p[...] = start[1]
    halo_copy.wait()

    @pl.when(sq == 0)
    def _():
        mix[0:8, :] = jnp.zeros((8, cw), F32)

    taps_own = taps[:, pl.ds(pl.multiple_of(me * cw, 128), cw)].astype(F32)
    hg_own = hgain[:, pl.ds(pl.multiple_of(me * heads * DV, 128), heads * DV)].astype(F32)
    reach = taps.shape[0] - 1
    width = out.shape[1]
    piece = 512

    def finish(r0, dst, d0):
        spot = pl.ds(r0, ch)
        window = mix[pl.ds(r0, ch + 8), :]
        summed = jnp.zeros((ch, cw), F32)
        for j in range(reach + 1):
            at = 8 - reach + j
            summed = summed + taps_own[j : j + 1] * window[at : at + ch]
        conv = (ao[spot, :].astype(F32) * summed).astype(BF)
        cells = []
        for h in range(heads):
            side = slice(h * DV, (h + 1) * DV)
            top = own_c[spot, 8 + h : 9 + h]
            lead = start_p[h : h + 1, 0:1]
            peak = jnp.maximum(top, lead)
            remote = jnp.dot(aq[spot, h * DQK : (h + 1) * DQK], start_s[h], preferred_element_type=F32)
            num = jnp.exp(lead - peak) * remote + jnp.exp(top - peak) * local[spot, side]
            num = num * lax.rsqrt(jnp.mean(num * num, axis=1, keepdims=True) + EPS)
            cells.append((num * hg_own[:, side] * jax.nn.sigmoid(ag[spot, side].astype(F32))).astype(BF))
        memory = jnp.concatenate(cells, axis=1)
        for w0 in range(0, width, piece):
            cols = slice(w0, w0 + piece)
            term = jnp.dot(conv, vco[:, cols], preferred_element_type=F32) + jnp.dot(
                memory, vmo[:, cols], preferred_element_type=F32
            )
            dst[pl.ds(d0, ch), cols] = term.astype(BF)

    def part_copy(k, c):
        spot = pl.ds(pl.multiple_of((k - 1) * own + c * ch, 8), ch)
        back = pl.ds(pl.multiple_of((n_tp - k - 1) * own + c * ch, 8), ch)
        return pltpu.make_async_remote_copy(
            src_ref=part_send.at[spot],
            dst_ref=part_recv.at[back],
            send_sem=psend.at[k - 1, c],
            recv_sem=precv.at[n_tp - k - 1, c],
            device_id={"tp": lax.rem(me + k, n_tp)},
            device_id_type=MESH,
        )

    def for_peer(step, carry):
        k = step // nch + 1
        c = step % nch
        owner = lax.rem(me + k, n_tp)
        finish(
            pl.multiple_of(owner * own + c * ch, 8), part_send, pl.multiple_of((k - 1) * own + c * ch, 8)
        )
        part_copy(k, c).start()
        return carry

    lax.fori_loop(0, (n_tp - 1) * nch, for_peer, 0)

    def for_self(c, carry):
        finish(pl.multiple_of(me * own + c * ch, 8), out, pl.multiple_of(c * ch, 8))
        return carry

    lax.fori_loop(0, nch, for_self, 0)

    def gather_parts(c, carry):
        spot = pl.ds(pl.multiple_of(c * ch, 8), ch)
        acc = out[spot, :].astype(F32)
        for k in range(1, n_tp):
            part_copy(k, c).wait_send()
            pltpu.make_async_remote_copy(
                src_ref=part_send.at[pl.ds(0, ch)],
                dst_ref=part_recv.at[pl.ds(pl.multiple_of((k - 1) * own + c * ch, 8), ch)],
                send_sem=psend.at[0, 0],
                recv_sem=precv.at[k - 1, c],
                device_id={"tp": lax.rem(me + k, n_tp)},
                device_id_type=MESH,
            ).wait_recv()
            acc = acc + part_recv[pl.ds(pl.multiple_of((k - 1) * own + c * ch, 8), ch), :].astype(F32)
        out[spot, :] = acc.astype(BF)
        return carry

    lax.fori_loop(0, nch, gather_parts, 0)


def on_device(n_sp, n_tp, *args):
    (tok, gain, wo, wi, ws, taps, wq, wk, wv, wg, gin, gfo, bin_, bfo, pos, extra, s0, p0, hgain, wco, wmo) = args
    own, width = tok.shape
    total = own * n_tp
    cw = wo.shape[1]
    qw = wq.shape[1]
    vw = wv.shape[1]
    heads = qw // DQK
    ch = 128 if own % 128 == 0 else own
    nch = own // ch
    rounds = n_sp.bit_length() - 1
    vm = pl.BlockSpec(memory_space=pltpu.VMEM)
    hbm = pl.BlockSpec(memory_space=pl.ANY)
    weights = (2, 3, 4, 6, 7, 8, 9, 19, 20)
    V = pltpu.VMEM
    sem = pltpu.SemaphoreType.DMA
    return pl.pallas_call(
        functools.partial(kernel, n_sp, n_tp),
        out_shape=jax.ShapeDtypeStruct((own, width), BF),
        in_specs=[hbm if i in weights else vm for i in range(21)],
        out_specs=vm,
        scratch_shapes=[
            V((total, width), BF),
            V(wo.shape, BF), V(wi.shape, BF), V(ws.shape, BF), V(wq.shape, BF), V(wk.shape, BF),
            V(wv.shape, BF), V(wg.shape, BF), V(wco.shape, BF), V(wmo.shape, BF),
            V((total, cw), BF), V((total + 8, cw), F32), V((total, qw), BF), V((total, qw), BF),
            V((total, vw), BF), V((total, vw), BF), V((total, 128), F32), V((128, total), F32),
            V((128, total), F32), V((total, 128), F32), V((total, vw), F32), V((8, cw), F32),
            V((rounds, heads, DQK, DV), BF), V((rounds, heads, DQK, DV), BF),
            V((rounds, 16, DV), F32), V((rounds, 16, DV), F32),
            V((heads, DQK, DV), BF), V((8, DV), F32),
            V(((n_tp - 1) * own, width), BF), V(((n_tp - 1) * own, width), BF),
            sem((9,)), sem((n_tp - 1, nch)), sem((n_tp - 1, nch)), sem((2,)),
            sem((rounds, 2)), sem((rounds, 2)), sem((n_tp - 1, nch)), sem((n_tp - 1, nch)),
        ],
        compiler_params=pltpu.CompilerParams(
            collective_id=0, has_side_effects=True, vmem_limit_bytes=62 * 1024 * 1024
        ),
    )(
        tok, gain[None], wo, wi, ws, taps, wq, wk, wv, wg, gin, gfo, bin_[None], bfo[None],
        pos[None], extra, s0, p0[None], hgain[None], wco, wmo,
    )


def solution(mesh):
    cols = P(None, "tp")
    in_specs = (
        P(("sp", "tp"), None), P(), cols, cols, cols, P(), cols, cols, cols, cols, P(), P(), P(), P(),
        P("sp"), P("sp", None), P(), P(), P(), P("tp", None), P("tp", None),
    )
    body = functools.partial(on_device, mesh.shape["sp"], mesh.shape["tp"])
    return jax.shard_map(
        body, mesh=mesh, in_specs=in_specs, out_specs=P(("sp", "tp"), None), check_vma=False
    )
```

time: 273 us -> 108 us (0.40)
  Pallas kernels: 0 us -> 96.2 us
  waiting for transfers between devices: 82.7 us -> 0 us
  matrix products: 56 us -> 0 us
  other arithmetic: 48.7 us -> 0 us
  blocking collectives: 32.5 us -> 0 us
  local copies, waits for them, and re-layouts: 35 us -> 11.8 us
  between operations: 14.3 us -> 0.01 us
    pallas_call x0 -> x1, Pallas kernels: none -> 96.2 us  [on_device(): pl.pallas_call(functools.partial(kernel, n_sp, n_tp), out_shape=jax.Shape...]
    dot_general x14 -> x0, matrix products: 56 us -> none  [the longest x5 15.2 us: project(): jnp.dot(normed, weight, preferred_element_type=jnp.float32)]
    all_gather x2 -> x0, waiting for transfers between devices: 42.2 us -> none  [the longest x1 42.1 us: on_device(): gathered = lax.all_gather(tokens, 'tp', axis=0, tiled=True)]
    reduce_scatter x1 -> x0, waiting for transfers between devices: 39.8 us -> none  [on_device(): lax.psum_scatter((jnp.dot(conv_out, convolution_output_weight, preferred_...]
    unnamed x1 -> x0, blocking collectives: 32.5 us -> none
    exp x18 -> x0, other arithmetic: 16.9 us -> none  [the longest x8 8.29 us: merge_states(): jnp.exp(lifted - ceiling)[..., None, None] * state_one]
    dynamic_update_slice x12 -> x0, local copies, waits for them, and re-layouts: 15.4 us -> none  [on_device(): lax.scan(advance, identity, (block_state, block_peak, block_total))]
    broadcast_in_dim x7 -> x0, other arithmetic: 6.85 us -> none  [on_device(): lax.scan(advance, identity, (block_state, block_peak, block_total))]
  transfers between devices with their start and end apart: 4 -> 0, of which waited for: 2 -> 0; matrix products, arithmetic and copies ran while one was open for 34% -> 0% of each run, Pallas kernels for 0% -> 0%
where the time goes in v1:
time: 108 us
  Pallas kernels  96.2 us (89%)
  local copies, waits for them, and re-layouts  11.8 us (11%)
    pallas_call x1, Pallas kernels, on_device(): pl.pallas_call(functools.partial(kernel, n_sp, n_tp), out_shape=jax.Shape...  96.2 us
    unnamed x4, local copies, waits for them, and re-layouts  7.93 us

profile of v1, /device:TPU:0, one launch (start us, length us, event | category | flops | bytes accessed | tf_op | source)
XLA Modules:
  0.0 108.0 jit_solution(8364175534341502607)
XLA Ops:
  0.0 1.3 %broadcast_in_dim.21.pos = f32[1,768]{1,0:T(1,128)} reshape(f32[768]{0:T(1024)} %param.35) | data formatting | bytes 6144 | tf_op jit(solution)/shard_map/broadcast_in_dim | solution.py:370
  1.3 1.3 %broadcast_in_dim.23.hgain = bf16[1,1024]{1,0:T(2,128)(2,1)} reshape(bf16[1024]{0:T(1024)(128)(2,1)} %param.39) | data formatting | bytes 4096 | tf_op jit(solution)/shard_map/broadcast_in_dim | solution.py:370
  2.5 1.3 %broadcast_in_dim.18.gain = bf16[1,2048]{1,0:T(2,128)(2,1)} reshape(bf16[2048]{0:T(1024)(128)(2,1)} %param.22) | data formatting | bytes 8192 | tf_op jit(solution)/shard_map/broadcast_in_dim | solution.py:369
  3.8 1.7 %copy.24.extra = f32[768,8]{1,0:T(8,128)} copy(f32[768,8]{0,1:T(8,128)} %param.36) | data formatting | bytes 49152 | tf_op args[15]
  5.5 1.8 %copy.22.gin = bf16[2048,8]{1,0:T(8,128)(2,1)} copy(bf16[2048,8]{0,1:T(8,128)(2,1)} %param.31) | data formatting | bytes 65536 | tf_op args[10]
  7.3 1.8 %copy.23.gfo = bf16[2048,8]{1,0:T(8,128)(2,1)} copy(bf16[2048,8]{0,1:T(8,128)(2,1)} %param.32) | data formatting | bytes 65536 | tf_op args[11]
  9.0 96.2 %shard_map.199 = bf16[384,2048]{1,0:T(8,128)(2,1)} custom-call(bf16[384,2048]{1,0:T(8,128)(2,1)} %tok.1, bf16[1,2048]{1,0:T(2,128)(2,1)} %broadcast_in_dim.18.gain, bf16[2048,512]{1,0:T(8,128)(2,1)} %wo.1, bf16[2048,512]{1,0:T(8,128)(2,1)} %wi.1, bf16[2048,512]{1,0:T(8,128)(2,1)} %ws.1, bf16[3,1024]{1,0:T(4,128)(2,1)} %taps.1, bf16[2048,256]{1,0:T(8,128)(2,1)} %wq.1, ...), custom_call_target="tpu_custom_call" | custom-call | tf_op jit(solution)/shard_map/pallas_call | solution.py:346
  105.3 2.7 %copy.26 = bf16[384,2048]{1,0:T(8,128)(2,1)} copy(bf16[384,2048]{1,0:T(8,128)(2,1)} %shard_map.199) | data formatting | bytes 3145728

commit v2 on v1

--- a/solution.py
+++ b/solution.py
@@ -26,6 +26,10 @@
     return x
 
 
+def exchanges_middle(n_sp, n_tp, own, depth):
+    return n_tp == 2 and n_sp % 4 == 0 and n_sp >= 8 and depth % (16 * n_sp) == 0 and own % 128 == 0
+
+
 def merge(earlier, later):
     s1, p1, d1 = earlier
     s2, p2, d2 = later
@@ -40,10 +44,12 @@
     n_sp, n_tp,
     tok, gain, wo, wi, ws, taps, wq, wk, wv, wg, gin, gfo, bin_, bfo, pos, extra, s0, p0, hgain, wco, wmo,
     out,
-    rows, vo, vi, vs, vq, vk, vv, vg, vco, vmo,
+    rows, vo, vi, vs, vq, vk, vv, vg, vown, vother,
     ao, mix, aq, ak, av, ag, gates, gates_t, own_t, own_c, local, halo_send,
     st_send, st_recv, sc_send, sc_recv, start_s, start_p, part_send, part_recv,
+    conv_own, conv_send, conv_recv, mem_own, mem_send, mem_recv, acc,
     wsem, tsend, trecv, hsem, ssend, srecv, psend, precv,
+    xsem, zsend, zrecv, ysend, yrecv, csend, crecv, cvsend, cvrecv,
 ):
     me = lax.axis_index("tp")
     sq = lax.axis_index("sp")
@@ -52,11 +58,16 @@
     ch = 128 if own % 128 == 0 else own
     nch = own // ch
     heads = aq.shape[1] // DQK
-    mh = gin.shape[1]
+    mh = gin.shape[0]
     cw = ao.shape[1]
+    vw = av.shape[1]
     rounds = n_sp.bit_length() - 1
-
-    pairs = [(wo, vo), (wi, vi), (ws, vs), (wq, vq), (wk, vk), (wv, vv), (wg, vg), (wco, vco), (wmo, vmo)]
+    middle = exchanges_middle(n_sp, n_tp, own, cw + vw)
+    far = n_sp // 4
+    bit_rows = (cw + vw) // n_sp
+    vco, vmo = vown.at[0:cw], vown.at[cw : cw + vw]
+
+    pairs = [(wco, vco), (wmo, vmo), (wo, vo), (wi, vi), (ws, vs), (wq, vq), (wk, vk), (wv, vv), (wg, vg)]
     loads = [pltpu.make_async_copy(src, dst, wsem.at[i]) for i, (src, dst) in enumerate(pairs)]
     for load in loads:
         load.start()
@@ -72,7 +83,65 @@
         pl.semaphore_signal(barrier, inc=1, device_id={"sp": partner(r)[1]}, device_id_type=MESH)
     pl.semaphore_signal(barrier, inc=1, device_id={"sp": lax.rem(sq + 1, n_sp)}, device_id_type=MESH)
     pl.semaphore_signal(barrier, inc=1, device_id={"sp": lax.rem(sq + n_sp - 1, n_sp)}, device_id_type=MESH)
-    pl.semaphore_wait(barrier, n_tp - 1 + rounds + 2)
+    greeted = n_tp - 1 + rounds + 2
+    if middle:
+        for k in range(1, far):
+            there = lax.rem(sq // 4 + k, far) * 4 + sq % 4
+            pl.semaphore_signal(barrier, inc=1, device_id={"sp": there}, device_id_type=MESH)
+        greeted += far - 1
+    pl.semaphore_wait(barrier, greeted)
+
+    def piece_of(index):
+        return pl.ds(pl.multiple_of(index * bit_rows, 16), bit_rows)
+
+    def relay(index, send, recv, device):
+        return pltpu.make_async_remote_copy(
+            src_ref=vother.at[piece_of(index)],
+            dst_ref=vother.at[piece_of(index)],
+            send_sem=send,
+            recv_sem=recv,
+            device_id=device,
+            device_id_type=MESH,
+        )
+
+    flip_y, flip_c = partner(1)[1], partner(0)[1]
+
+    def z_index(k):
+        return lax.rem(sq // 4 + k, far) * 4 + sq % 4
+
+    def z_send(k):
+        return relay(sq, zsend.at[k - 1], zrecv.at[far - k - 1], {"sp": z_index(k)})
+
+    def z_arrive(k):
+        return relay(z_index(k), zsend.at[k - 1], zrecv.at[k - 1], {"sp": z_index(k)})
+
+    def y_send(k):
+        return relay(z_index(k), ysend.at[k], yrecv.at[k], {"sp": flip_y})
+
+    def y_arrive(k):
+        return relay(lax.rem(sq // 4 + k, far) * 4 + flip_y % 4, ysend.at[k], yrecv.at[k], {"sp": flip_y})
+
+    def c_send(k):
+        index = z_index(k) if k < far else lax.rem(sq // 4 + k - far, far) * 4 + flip_y % 4
+        return relay(index, csend.at[k], crecv.at[k], {"sp": flip_c})
+
+    def c_arrive(k):
+        low = flip_c % 4 if k < far else 3 - sq % 4
+        index = lax.rem(sq // 4 + k % far, far) * 4 + low
+        return relay(index, csend.at[k], crecv.at[k], {"sp": flip_c})
+
+    if middle:
+        loads[0].wait()
+        loads[1].wait()
+        cross = pltpu.make_async_remote_copy(
+            src_ref=vown.at[piece_of(sq)],
+            dst_ref=vother.at[piece_of(sq)],
+            send_sem=xsem.at[0],
+            recv_sem=xsem.at[1],
+            device_id={"tp": 1 - me},
+            device_id_type=MESH,
+        )
+        cross.start()
 
     def token_copy(k, c):
         return pltpu.make_async_remote_copy(
@@ -88,7 +157,7 @@
     for copy in sends:
         copy.start()
     rows[pl.ds(pl.multiple_of(me * own, 8), own), :] = tok[...]
-    for load in loads:
+    for load in loads[2 if middle else 0 :]:
         load.wait()
     gates[...] = jnp.zeros_like(gates)
     own_t[...] = jnp.zeros_like(own_t)
@@ -99,6 +168,23 @@
         owner = lax.rem(me + k, n_tp)
         r0 = pl.multiple_of(owner * own + c * ch, 8)
         spot = pl.ds(r0, ch)
+
+        if middle:
+
+            @pl.when(step == nch)
+            def _():
+                cross.wait_recv()
+                for j in range(1, far):
+                    z_send(j).start()
+                y_send(0).start()
+
+            @pl.when(step == 2 * nch - 1)
+            def _():
+                for j in range(1, far):
+                    z_arrive(j).wait_recv()
+                    y_send(j).start()
+                for j in range(far):
+                    c_send(j).start()
 
         @pl.when(step >= nch)
         def _():
@@ -118,10 +204,12 @@
         def dot(w):
             return jnp.dot(normed, w[...], preferred_element_type=F32)
 
-        gates[spot, 0:mh] = dot(gfo) + bfo[...]
-        gates[spot, mh : 2 * mh] = dot(gin) + bin_[...]
-        gates[spot, 2 * mh : 3 * mh] = extra[spot, :]
-        gates[spot, 3 * mh : 4 * mh] = jnp.broadcast_to(p0[...], (ch, mh))
+        def dot_t(w):
+            return lax.dot_general(normed, w[...], (((1,), (1,)), ((), ())), preferred_element_type=F32)
+
+        gates[spot, 0:mh] = dot_t(gfo) + bfo[...]
+        gates[spot, mh : 2 * mh] = dot_t(gin) + bin_[...]
+        gates[spot, 2 * mh : 3 * mh] = jnp.broadcast_to(p0[...], (ch, mh))
         aq[spot, :] = (dot(vq) * DQK ** -0.5).astype(BF)
         ak[spot, :] = dot(vk).astype(BF)
         av[spot, :] = dot(vv).astype(BF)
@@ -149,14 +237,14 @@
 
     gates_t[...] = gates[...].T
 
-    def own_rows(group):
-        picked = [gates_t[pl.ds(group * mh + me * heads + h, 1), :] for h in range(heads)]
+    def own_rows(group, source=gates_t):
+        picked = [source[pl.ds(group * mh + me * heads + h, 1), :] for h in range(heads)]
         picked += [jnp.zeros((8 - heads, total), F32)] if heads < 8 else []
         return jnp.concatenate(picked, axis=0)
 
     pre = own_rows(0)
     log_sig = jnp.minimum(pre, 0.0) - jnp.log1p(jnp.exp(-jnp.abs(pre)))
-    log_forget = pos[...] * log_sig + own_rows(2)
+    log_forget = pos[...] * log_sig + own_rows(0, extra)
     cumul = scan_lanes(log_forget, jnp.add, 0.0)
     lifted_in = own_rows(1) - cumul
     running = scan_lanes(lifted_in, jnp.maximum, FLOOR_LOG)
@@ -197,6 +285,39 @@
             local[lo:end, h * DV : (h + 1) * DV] = jnp.dot(
                 weighted, av[0:end, h * DV : (h + 1) * DV], preferred_element_type=F32
             )
+
+    taps_own = taps[:, pl.ds(pl.multiple_of(me * cw, 128), cw)].astype(F32)
+    hg_own = hgain[:, pl.ds(pl.multiple_of(me * heads * DV, 128), heads * DV)].astype(F32)
+    reach = taps.shape[0] - 1
+
+    def conv_rows(r0):
+        window = mix[pl.ds(r0, ch + 8), :]
+        summed = jnp.zeros((ch, cw), F32)
+        for j in range(reach + 1):
+            at = 8 - reach + j
+            summed = summed + taps_own[j : j + 1] * window[at : at + ch]
+        return (ao[pl.ds(r0, ch), :].astype(F32) * summed).astype(BF)
+
+    def mid_copy(src, dst, send, recv, c):
+        rows_c = pl.ds(pl.multiple_of(c * ch, 8), ch)
+        return pltpu.make_async_remote_copy(
+            src_ref=src.at[rows_c], dst_ref=dst.at[rows_c], send_sem=send, recv_sem=recv,
+            device_id={"tp": 1 - me}, device_id_type=MESH,
+        )
+
+    def conv_all():
+        def one(c, carry):
+            rows_c = pl.ds(pl.multiple_of(c * ch, 8), ch)
+            conv_send[rows_c, :] = conv_rows(pl.multiple_of((1 - me) * own + c * ch, 8))
+            mid_copy(conv_send, conv_recv, cvsend.at[c], cvrecv.at[c], c).start()
+            return carry
+
+        def two(c, carry):
+            conv_own[pl.ds(pl.multiple_of(c * ch, 8), ch), :] = conv_rows(pl.multiple_of(me * own + c * ch, 8))
+            return carry
+
+        lax.fori_loop(0, nch, one, 0)
+        lax.fori_loop(0, nch, two, 0)
 
     done = 0
     for r in range(rounds):
@@ -214,10 +335,23 @@
         ]
         for copy in copies:
             copy.start()
+        if r == 0:
+            halo_copy.wait()
+
+            @pl.when(sq == 0)
+            def _():
+                mix[0:8, :] = jnp.zeros((8, cw), F32)
+
+            if middle:
+                conv_all()
         want = heads if r == rounds - 1 else -(-heads * (r + 1) // rounds)
         while done < want:
             local_part(done)
             done += 1
+        if middle and r == rounds - 1:
+            for k in range(far):
+                y_arrive(k).wait_recv()
+                c_send(far + k).start()
         for copy in copies:
             copy.wait()
         theirs = ([st_recv[r, h].astype(F32) for h in range(heads)], sc_recv[r, 0:8], sc_recv[r, 8:16])
@@ -232,33 +366,28 @@
 
     first = (
         [s0[me * heads + h] for h in range(heads)],
-        own_rows(3)[:, 0:DV],
+        own_rows(2)[:, 0:DV],
         jnp.zeros((8, DV), F32),
     )
     start = merge(first, before)
     for h in range(heads):
         start_s[h] = start[0][h].astype(BF)
     start_p[...] = start[1]
-    halo_copy.wait()
-
-    @pl.when(sq == 0)
-    def _():
-        mix[0:8, :] = jnp.zeros((8, cw), F32)
-
-    taps_own = taps[:, pl.ds(pl.multiple_of(me * cw, 128), cw)].astype(F32)
-    hg_own = hgain[:, pl.ds(pl.multiple_of(me * heads * DV, 128), heads * DV)].astype(F32)
-    reach = taps.shape[0] - 1
     width = out.shape[1]
     piece = 512
 
     def finish(r0, dst, d0):
+        conv = conv_rows(r0)
+        memory = memory_rows(r0)
+        for w0 in range(0, width, piece):
+            cols = slice(w0, w0 + piece)
+            term = jnp.dot(conv, vown[0:cw, cols], preferred_element_type=F32) + jnp.dot(
+                memory, vown[cw : cw + vw, cols], preferred_element_type=F32
+            )
+            dst[pl.ds(d0, ch), cols] = term.astype(BF)
+
+    def memory_rows(r0):
         spot = pl.ds(r0, ch)
-        window = mix[pl.ds(r0, ch + 8), :]
-        summed = jnp.zeros((ch, cw), F32)
-        for j in range(reach + 1):
-            at = 8 - reach + j
-            summed = summed + taps_own[j : j + 1] * window[at : at + ch]
-        conv = (ao[spot, :].astype(F32) * summed).astype(BF)
         cells = []
         for h in range(heads):
             side = slice(h * DV, (h + 1) * DV)
@@ -269,13 +398,59 @@
             num = jnp.exp(lead - peak) * remote + jnp.exp(top - peak) * local[spot, side]
             num = num * lax.rsqrt(jnp.mean(num * num, axis=1, keepdims=True) + EPS)
             cells.append((num * hg_own[:, side] * jax.nn.sigmoid(ag[spot, side].astype(F32))).astype(BF))
-        memory = jnp.concatenate(cells, axis=1)
-        for w0 in range(0, width, piece):
-            cols = slice(w0, w0 + piece)
-            term = jnp.dot(conv, vco[:, cols], preferred_element_type=F32) + jnp.dot(
-                memory, vmo[:, cols], preferred_element_type=F32
-            )
-            dst[pl.ds(d0, ch), cols] = term.astype(BF)
+        return jnp.concatenate(cells, axis=1)
+
+    if middle:
+        peer0, own0 = (1 - me) * own, me * own
+
+        def memory_peer(c, carry):
+            rows_c = pl.ds(pl.multiple_of(c * ch, 8), ch)
+            mem_send[rows_c, :] = memory_rows(pl.multiple_of(peer0 + c * ch, 8))
+            mid_copy(mem_send, mem_recv, psend.at[0, c], precv.at[0, c], c).start()
+            return carry
+
+        lax.fori_loop(0, nch, memory_peer, 0)
+        for k in range(2 * far):
+            c_arrive(k).wait_recv()
+
+        def own_terms(c, carry):
+            rows_c = pl.ds(pl.multiple_of(c * ch, 8), ch)
+            conv = conv_own[rows_c, :]
+            mid_copy(conv_send, conv_recv, cvsend.at[c], cvrecv.at[c], c).wait()
+            other = conv_recv[rows_c, :]
+            memory = memory_rows(pl.multiple_of(own0 + c * ch, 8))
+            for w0 in range(0, width, piece):
+                cols = slice(w0, w0 + piece)
+                acc[rows_c, cols] = (
+                    jnp.dot(conv, vown[0:cw, cols], preferred_element_type=F32)
+                    + jnp.dot(other, vother[0:cw, cols], preferred_element_type=F32)
+                    + jnp.dot(memory, vown[cw : cw + vw, cols], preferred_element_type=F32)
+                )
+            return carry
+
+        lax.fori_loop(0, nch, own_terms, 0)
+
+        def last_terms(c, carry):
+            rows_c = pl.ds(pl.multiple_of(c * ch, 8), ch)
+            mid_copy(mem_send, mem_recv, psend.at[0, c], precv.at[0, c], c).wait()
+            memory = mem_recv[rows_c, :]
+            for w0 in range(0, width, piece):
+                cols = slice(w0, w0 + piece)
+                out[rows_c, cols] = (
+                    acc[rows_c, cols]
+                    + jnp.dot(memory, vother[cw : cw + vw, cols], preferred_element_type=F32)
+                ).astype(BF)
+            return carry
+
+        lax.fori_loop(0, nch, last_terms, 0)
+        cross.wait_send()
+        for k in range(1, far):
+            z_send(k).wait_send()
+        for k in range(far):
+            y_send(k).wait_send()
+        for k in range(2 * far):
+            c_send(k).wait_send()
+        return
 
     def part_copy(k, c):
         spot = pl.ds(pl.multiple_of((k - 1) * own + c * ch, 8), ch)
@@ -338,6 +513,8 @@
     ch = 128 if own % 128 == 0 else own
     nch = own // ch
     rounds = n_sp.bit_length() - 1
+    middle = exchanges_middle(n_sp, n_tp, own, cw + vw)
+    far = max(n_sp // 4, 1)
     vm = pl.BlockSpec(memory_space=pltpu.VMEM)
     hbm = pl.BlockSpec(memory_space=pl.ANY)
     weights = (2, 3, 4, 6, 7, 8, 9, 19, 20)
@@ -351,23 +528,26 @@
         scratch_shapes=[
             V((total, width), BF),
             V(wo.shape, BF), V(wi.shape, BF), V(ws.shape, BF), V(wq.shape, BF), V(wk.shape, BF),
-            V(wv.shape, BF), V(wg.shape, BF), V(wco.shape, BF), V(wmo.shape, BF),
+            V(wv.shape, BF), V(wg.shape, BF), V((cw + vw, width), BF), V((cw + vw if middle else 16, width), BF),
             V((total, cw), BF), V((total + 8, cw), F32), V((total, qw), BF), V((total, qw), BF),
             V((total, vw), BF), V((total, vw), BF), V((total, 128), F32), V((128, total), F32),
             V((128, total), F32), V((total, 128), F32), V((total, vw), F32), V((8, cw), F32),
             V((rounds, heads, DQK, DV), BF), V((rounds, heads, DQK, DV), BF),
             V((rounds, 16, DV), F32), V((rounds, 16, DV), F32),
             V((heads, DQK, DV), BF), V((8, DV), F32),
-            V(((n_tp - 1) * own, width), BF), V(((n_tp - 1) * own, width), BF),
+            V((16 if middle else (n_tp - 1) * own, width), BF), V((16 if middle else (n_tp - 1) * own, width), BF),
+            *[V((own if middle else 16, cw), BF)] * 3, *[V((own if middle else 16, vw), BF)] * 3,
+            V((own if middle else 8, width), F32),
             sem((9,)), sem((n_tp - 1, nch)), sem((n_tp - 1, nch)), sem((2,)),
             sem((rounds, 2)), sem((rounds, 2)), sem((n_tp - 1, nch)), sem((n_tp - 1, nch)),
+            sem((2,)), sem((far,)), sem((far,)), sem((far,)), sem((far,)), sem((2 * far,)), sem((2 * far,)), sem((nch,)), sem((nch,)),
         ],
         compiler_params=pltpu.CompilerParams(
             collective_id=0, has_side_effects=True, vmem_limit_bytes=62 * 1024 * 1024
         ),
     )(
-        tok, gain[None], wo, wi, ws, taps, wq, wk, wv, wg, gin, gfo, bin_[None], bfo[None],
-        pos[None], extra, s0, p0[None], hgain[None], wco, wmo,
+        tok, gain.reshape(1, -1), wo, wi, ws, taps, wq, wk, wv, wg, gin.T, gfo.T, bin_.reshape(1, -1),
+        bfo.reshape(1, -1), pos.reshape(1, -1), extra.T, s0, p0.reshape(1, -1), hgain.reshape(1, -1), wco, wmo,
     )
 
 

time: 108 us -> 86 us (0.80)
  Pallas kernels: 96.2 us -> 79.2 us
  local copies, waits for them, and re-layouts: 11.8 us -> 6.56 us
    pallas_call x1, Pallas kernels: 96.2 us -> 79.2 us  [on_device(): pl.pallas_call(functools.partial(kernel, n_sp, n_tp), out_shape=jax.Shape...]
    unnamed x4 -> x1, local copies, waits for them, and re-layouts: 7.93 us -> 2.73 us
    reshape x0 -> x3, local copies, waits for them, and re-layouts: none -> 3.83 us  [the longest x1 1.29 us: on_device(): gain.reshape(1, -1)]
    broadcast_in_dim x3 -> x0, local copies, waits for them, and re-layouts: 3.83 us -> none  [the longest x1 1.29 us: on_device(): gain[None]]
where the time goes in v2:
time: 86 us; the launch traced here: 85.8 us
  Pallas kernels  79.2 us (92%)
  local copies, waits for them, and re-layouts  6.56 us (8%)
    pallas_call x1, Pallas kernels, on_device(): pl.pallas_call(functools.partial(kernel, n_sp, n_tp), out_shape=jax.Shape...  79.2 us
    unnamed x1, local copies, waits for them, and re-layouts  2.73 us

profile of v2, /device:TPU:0, one launch (start us, length us, event | category | flops | bytes accessed | tf_op | source)
XLA Modules:
  0.0 85.8 jit_solution(18393492278619309630)
XLA Ops:
  0.0 1.3 %reshape.21.pos = f32[1,768]{1,0:T(1,128)} reshape(f32[768]{0:T(1024)} %param.35) | data formatting | bytes 6144 | tf_op jit(solution)/shard_map/reshape | solution.py:550
  1.3 1.3 %reshape.23.hgain = bf16[1,1024]{1,0:T(2,128)(2,1)} reshape(bf16[1024]{0:T(1024)(128)(2,1)} %param.39) | data formatting | bytes 4096 | tf_op jit(solution)/shard_map/reshape | solution.py:550
  2.5 1.3 %reshape.18.gain = bf16[1,2048]{1,0:T(2,128)(2,1)} reshape(bf16[2048]{0:T(1024)(128)(2,1)} %param.22) | data formatting | bytes 8192 | tf_op jit(solution)/shard_map/reshape | solution.py:549
  3.8 79.2 %shard_map.199 = bf16[384,2048]{1,0:T(8,128)(2,1)} custom-call(bf16[384,2048]{1,0:T(8,128)(2,1)} %tok.1, bf16[1,2048]{1,0:T(2,128)(2,1)} %reshape.18.gain, bf16[2048,512]{1,0:T(8,128)(2,1)} %wo.1, bf16[2048,512]{1,0:T(8,128)(2,1)} %wi.1, bf16[2048,512]{1,0:T(8,128)(2,1)} %ws.1, bf16[3,1024]{1,0:T(4,128)(2,1)} %taps.1, bf16[2048,256]{1,0:T(8,128)(2,1)} %wq.1, ...), custom_call_target="tpu_custom_call" | custom-call | tf_op jit(solution)/shard_map/pallas_call | solution.py:523
  83.0 2.7 %copy.23 = bf16[384,2048]{1,0:T(8,128)(2,1)} copy(bf16[384,2048]{1,0:T(8,128)(2,1)} %shard_map.199) | data formatting | bytes 3145728

commit v3 on v2

--- a/solution.py
+++ b/solution.py
@@ -26,8 +26,13 @@
     return x
 
 
-def exchanges_middle(n_sp, n_tp, own, depth):
-    return n_tp == 2 and n_sp % 4 == 0 and n_sp >= 8 and depth % (16 * n_sp) == 0 and own % 128 == 0
+def exchanges_middle(n_sp, n_tp, own, cw, depth):
+    return n_tp == 2 and n_sp % 4 == 0 and n_sp >= 8 and cw % (depth // n_sp) == 0 and depth % (16 * n_sp) == 0 and own % 128 == 0
+
+
+def flat(ref):
+    rows = ref[...].astype(F32)
+    return jnp.concatenate([rows[i : i + 1] for i in range(rows.shape[0])], axis=1)
 
 
 def merge(earlier, later):
@@ -47,7 +52,7 @@
     rows, vo, vi, vs, vq, vk, vv, vg, vown, vother,
     ao, mix, aq, ak, av, ag, gates, gates_t, own_t, own_c, local, halo_send,
     st_send, st_recv, sc_send, sc_recv, start_s, start_p, part_send, part_recv,
-    conv_own, conv_send, conv_recv, mem_own, mem_send, mem_recv, acc,
+    gain_row, hg_rows, conv_own, conv_send, conv_recv, mem_own, mem_send, mem_recv, acc,
     wsem, tsend, trecv, hsem, ssend, srecv, psend, precv,
     xsem, zsend, zrecv, ysend, yrecv, csend, crecv, cvsend, cvrecv,
 ):
@@ -62,12 +67,12 @@
     cw = ao.shape[1]
     vw = av.shape[1]
     rounds = n_sp.bit_length() - 1
-    middle = exchanges_middle(n_sp, n_tp, own, cw + vw)
+    middle = exchanges_middle(n_sp, n_tp, own, cw, cw + vw)
     far = n_sp // 4
     bit_rows = (cw + vw) // n_sp
     vco, vmo = vown.at[0:cw], vown.at[cw : cw + vw]
 
-    pairs = [(wco, vco), (wmo, vmo), (wo, vo), (wi, vi), (ws, vs), (wq, vq), (wk, vk), (wv, vv), (wg, vg)]
+    pairs = [(wq, vq), (wk, vk), (wv, vv), (wg, vg), (wo, vo), (wi, vi), (ws, vs), (wco, vco), (wmo, vmo)]
     loads = [pltpu.make_async_copy(src, dst, wsem.at[i]) for i, (src, dst) in enumerate(pairs)]
     for load in loads:
         load.start()
@@ -130,18 +135,27 @@
         index = lax.rem(sq // 4 + k % far, far) * 4 + low
         return relay(index, csend.at[k], crecv.at[k], {"sp": flip_c})
 
-    if middle:
-        loads[0].wait()
-        loads[1].wait()
-        cross = pltpu.make_async_remote_copy(
-            src_ref=vown.at[piece_of(sq)],
+    def cross_copy(src, index):
+        return pltpu.make_async_remote_copy(
+            src_ref=src.at[piece_of(index)],
             dst_ref=vother.at[piece_of(sq)],
             send_sem=xsem.at[0],
             recv_sem=xsem.at[1],
             device_id={"tp": 1 - me},
             device_id_type=MESH,
         )
-        cross.start()
+
+    if middle:
+        cross = cross_copy(wco, 0)
+        split = cw // bit_rows
+
+        @pl.when(sq < split)
+        def _():
+            cross_copy(wco, sq).start()
+
+        @pl.when(sq >= split)
+        def _():
+            cross_copy(wmo, sq - split).start()
 
     def token_copy(k, c):
         return pltpu.make_async_remote_copy(
@@ -157,8 +171,10 @@
     for copy in sends:
         copy.start()
     rows[pl.ds(pl.multiple_of(me * own, 8), own), :] = tok[...]
-    for load in loads[2 if middle else 0 :]:
+    for load in loads:
         load.wait()
+    gain_row[...] = flat(gain)
+    hg_rows[...] = hgain[...].astype(F32)
     gates[...] = jnp.zeros_like(gates)
     own_t[...] = jnp.zeros_like(own_t)
 
@@ -199,7 +215,7 @@
 
         wide = rows[spot, :].astype(F32)
         scale = lax.rsqrt(jnp.mean(wide * wide, axis=1, keepdims=True) + EPS)
-        normed = (wide * scale * gain[...].astype(F32)).astype(BF)
+        normed = (wide * scale * gain_row[...]).astype(BF)
 
         def dot(w):
             return jnp.dot(normed, w[...], preferred_element_type=F32)
@@ -244,7 +260,7 @@
 
     pre = own_rows(0)
     log_sig = jnp.minimum(pre, 0.0) - jnp.log1p(jnp.exp(-jnp.abs(pre)))
-    log_forget = pos[...] * log_sig + own_rows(0, extra)
+    log_forget = flat(pos) * log_sig + own_rows(0, extra)
     cumul = scan_lanes(log_forget, jnp.add, 0.0)
     lifted_in = own_rows(1) - cumul
     running = scan_lanes(lifted_in, jnp.maximum, FLOOR_LOG)
@@ -287,7 +303,6 @@
             )
 
     taps_own = taps[:, pl.ds(pl.multiple_of(me * cw, 128), cw)].astype(F32)
-    hg_own = hgain[:, pl.ds(pl.multiple_of(me * heads * DV, 128), heads * DV)].astype(F32)
     reach = taps.shape[0] - 1
 
     def conv_rows(r0):
@@ -397,7 +412,7 @@
             remote = jnp.dot(aq[spot, h * DQK : (h + 1) * DQK], start_s[h], preferred_element_type=F32)
             num = jnp.exp(lead - peak) * remote + jnp.exp(top - peak) * local[spot, side]
             num = num * lax.rsqrt(jnp.mean(num * num, axis=1, keepdims=True) + EPS)
-            cells.append((num * hg_own[:, side] * jax.nn.sigmoid(ag[spot, side].astype(F32))).astype(BF))
+            cells.append((num * hg_rows[pl.ds(me * heads + h, 1), :] * jax.nn.sigmoid(ag[spot, side].astype(F32))).astype(BF))
         return jnp.concatenate(cells, axis=1)
 
     if middle:
@@ -513,7 +528,7 @@
     ch = 128 if own % 128 == 0 else own
     nch = own // ch
     rounds = n_sp.bit_length() - 1
-    middle = exchanges_middle(n_sp, n_tp, own, cw + vw)
+    middle = exchanges_middle(n_sp, n_tp, own, cw, cw + vw)
     far = max(n_sp // 4, 1)
     vm = pl.BlockSpec(memory_space=pltpu.VMEM)
     hbm = pl.BlockSpec(memory_space=pl.ANY)
@@ -536,6 +551,7 @@
             V((rounds, 16, DV), F32), V((rounds, 16, DV), F32),
             V((heads, DQK, DV), BF), V((8, DV), F32),
             V((16 if middle else (n_tp - 1) * own, width), BF), V((16 if middle else (n_tp - 1) * own, width), BF),
+            V((1, width), F32), V((hgain.shape[0] // DV, DV), F32),
             *[V((own if middle else 16, cw), BF)] * 3, *[V((own if middle else 16, vw), BF)] * 3,
             V((own if middle else 8, width), F32),
             sem((9,)), sem((n_tp - 1, nch)), sem((n_tp - 1, nch)), sem((2,)),
@@ -546,8 +562,8 @@
             collective_id=0, has_side_effects=True, vmem_limit_bytes=62 * 1024 * 1024
         ),
     )(
-        tok, gain.reshape(1, -1), wo, wi, ws, taps, wq, wk, wv, wg, gin.T, gfo.T, bin_.reshape(1, -1),
-        bfo.reshape(1, -1), pos.reshape(1, -1), extra.T, s0, p0.reshape(1, -1), hgain.reshape(1, -1), wco, wmo,
+        tok, gain.reshape(-1, 128), wo, wi, ws, taps, wq, wk, wv, wg, gin.T, gfo.T, bin_.reshape(1, -1),
+        bfo.reshape(1, -1), pos.reshape(-1, 128), extra.T, s0, p0.reshape(1, -1), hgain.reshape(-1, DV), wco, wmo,
     )
 
 

time: 86 us -> 82 us (0.953)
  local copies, waits for them, and re-layouts: 6.56 us -> 2.73 us
    reshape x3 -> x0, local copies, waits for them, and re-layouts: 3.83 us -> none  [the longest x1 1.29 us: on_device(): gain.reshape(1, -1)]
where the time goes in v3:
time: 82 us; the launch traced here: 81.9 us
  Pallas kernels  79.1 us (96%)
  local copies, waits for them, and re-layouts  2.73 us (3%)
    pallas_call x1, Pallas kernels, on_device(): pl.pallas_call(functools.partial(kernel, n_sp, n_tp), out_shape=jax.Shape...  79.1 us
    unnamed x1, local copies, waits for them, and re-layouts  2.73 us

profile of v3, /device:TPU:0, one launch (start us, length us, event | category | flops | bytes accessed | tf_op | source)
XLA Modules:
  0.0 81.9 jit_solution(8449301923579950904)
XLA Ops:
  0.0 79.1 %shard_map.199 = bf16[384,2048]{1,0:T(8,128)(2,1)} custom-call(bf16[384,2048]{1,0:T(8,128)(2,1)} %tok.1, bf16[16,128]{1,0:T(8,128)(2,1)} %bitcast.12, bf16[2048,512]{1,0:T(8,128)(2,1)} %wo.1, bf16[2048,512]{1,0:T(8,128)(2,1)} %wi.1, bf16[2048,512]{1,0:T(8,128)(2,1)} %ws.1, bf16[3,1024]{1,0:T(4,128)(2,1)} %taps.1, bf16[2048,256]{1,0:T(8,128)(2,1)} %wq.1, ...), custom_call_target="tpu_custom_call" | custom-call | tf_op jit(solution)/shard_map/pallas_call | solution.py:538
  79.2 2.7 %copy.23 = bf16[384,2048]{1,0:T(8,128)(2,1)} copy(bf16[384,2048]{1,0:T(8,128)(2,1)} %shard_map.199) | data formatting | bytes 3145728
